TPU v7x, 32 devices: a whole 2x2x4 slice. The times are simulated.
32 devices in a mesh: grp: 2 (over y), sp: 4 (over z), tp: 4 (over x, core).
Axes of the slice: x: 2, y: 2, z: 4, core: 2. Of those that a mesh axis runs over, the one named last changes fastest.
Arguments:
- tokens: bfloat16 [16384, 2048], P(('grp', 'sp')), parts along dimension 0, may hold values from -6 to 6
- in_gain: float32 [2048], replicated, may hold values from 0.1 to 1.9
- w_input: bfloat16 [2048, 2048], P(None, 'tp'), may hold values from -0.125 to 0.125
- w_gate: bfloat16 [2048, 2048], P(None, 'tp'), may hold values from -4 to 4
- conv_taps: float32 [4, 2048], P(None, 'tp'), may hold values from -3 to 3
- w_rate: bfloat16 [8, 256, 256], P('tp'), may hold values from -0.375 to 0.375
- w_inlet: bfloat16 [8, 256, 256], P('tp'), may hold values from -0.375 to 0.375
- decay_param: float32 [2048], P('tp'), may hold values from 3 to 25
- decay_bias: float32 [8, 16384], P('tp', ('grp', 'sp')), parts along dimension 1, may hold values from -1.5 to 0
- out_gain: float32 [2048], P('tp'), may hold values from 0.1 to 1.9
- w_out: bfloat16 [2048, 2048], P('sp'), may hold values from -0.125 to 0.125
Outputs:
- mixer_out: bfloat16 [16384, 2048], P(('grp', 'sp', 'tp')), parts along dimension 0
There are 2 independent parts, one for each index of `grp`. A program takes and returns all parts, laid end to end along the dimension named above; an argument that names none is the same for every part. Nothing has to cross between parts.
All inputs are finite; a program needn't handle non-finite values.
Results may differ from a plain program's by a relative error of at most 0.013.
Values may be sent and summed in bfloat16 or wider, within the bound.
A program may use at most 128 MiB of HBM per device.

v0:
```python
import functools
import math
import jax
import jax.numpy as jnp
from jax import lax
from jax.experimental import pallas as pl
from jax.experimental.pallas import tpu as pltpu
from jax.sharding import PartitionSpec as P

MESH = pl.DeviceIdType.MESH
F32 = jnp.float32
BF16 = jnp.bfloat16
CHUNK = 256
SUB = 32


def normalize(raw, gain):
    as_float = raw.astype(F32)
    inv = lax.rsqrt(jnp.mean(as_float * as_float, axis=1, keepdims=True) + 1e-06)
    return (as_float * inv * gain).astype(BF16)


LN4 = 2.0 * math.log(2.0)
GELU_A = math.sqrt(2.0 / math.pi)
GELU_B = GELU_A * 0.044715


def one_minus_square(log2_decay, decay):
    a1, a2, a3, a4 = -LN4, -(LN4**2) / 2, -(LN4**3) / 6, -(LN4**4) / 24
    series = log2_decay * (a1 + log2_decay * (a2 + log2_decay * (a3 + log2_decay * a4)))
    return jnp.where(log2_decay > -0.025, series, 1.0 - decay * decay)


def gelu_half(value):
    inner = value * (GELU_A + GELU_B * (value * value))
    return (0.25 * value) * (1.0 + jnp.tanh(inner))


def kernel(
    sizes,
    tokens, in_gain, w_input, w_gate, taps, w_rate, w_inlet, rate_scale, bias, out_gain, w_out,
    out,
    x, wi, wg, w_all, state, prod, gate, gated, arrived, total, result, halo, padded, conv,
    halved, rate_in, inlet_in, squares, squares_in, ends, ends_in,
    x_sem, load_sem, halo_send, halo_recv, z_send, z_recv, x_send, x_recv, y_send, y_recv,
    c_send, c_recv,
    end_send, end_recv, a_send, a_recv, q_send, q_recv, own_sem, out_sem,
):
    n_grp, n_sp, n_tp = sizes
    grp, sp, tp = lax.axis_index("grp"), lax.axis_index("sp"), lax.axis_index("tp")
    rows, width = tokens.shape
    heads, head = w_rate.shape[0], w_rate.shape[1]
    reach = taps.shape[0] - 1
    chunks = rows // CHUNK
    out_rows = rows // n_tp
    shard = w_out.shape[0]
    piece = shard // (2 * n_grp * 2)
    core = lax.rem(tp, 2)
    mate = tp + 1 - 2 * core
    side = lax.rem(tp // 2, 2)
    beside = tp + 2 - 4 * side
    across = 1 - grp
    part = (core * n_grp + grp) * 2 + side
    part_beside = (core * n_grp + grp) * 2 + 1 - side

    def x_copy(i):
        at = pl.ds(pl.multiple_of(i * CHUNK, CHUNK), CHUNK)
        return pltpu.make_async_copy(tokens.at[at], x.at[at], x_sem.at[i])

    loads = [
        pltpu.make_async_copy(w_input, wi, load_sem.at[0]),
        pltpu.make_async_copy(w_gate, wg, load_sem.at[1]),
        pltpu.make_async_copy(
            w_out, w_all.at[pl.ds(pl.multiple_of(sp * shard, shard), shard)], load_sem.at[2]
        ),
    ]
    loads[0].start()
    x_copy(0).start()
    loads[1].start()
    for i in range(1, chunks):
        x_copy(i).start()
    loads[2].start()

    barrier = pltpu.get_barrier_semaphore()
    for d in range(1, n_sp):
        pl.semaphore_signal(
            barrier, inc=1, device_id={"sp": lax.rem(sp + d, n_sp)}, device_id_type=MESH
        )
    for k in range(1, n_tp):
        pl.semaphore_signal(
            barrier, inc=1, device_id={"tp": lax.rem(tp + k, n_tp)}, device_id_type=MESH
        )
    pl.semaphore_signal(barrier, inc=1, device_id={"grp": across}, device_id_type=MESH)
    pl.semaphore_wait(barrier, n_sp - 1 + n_tp - 1 + 1)

    def remote(src, dst, send, recv, where):
        return pltpu.make_async_remote_copy(
            src_ref=src, dst_ref=dst, send_sem=send, recv_sem=recv,
            device_id=where, device_id_type=MESH,
        )

    halo_rows = halo.shape[0]
    halo_copy = remote(
        tokens.at[pl.ds(rows - halo_rows, halo_rows)], halo, halo_send, halo_recv,
        {"sp": lax.rem(sp + 1, n_sp)},
    )
    halo_copy.start()

    def w_rows(d, which, count=1):
        source = lax.rem(sp + n_sp - d, n_sp)
        first = pl.multiple_of(source * shard + which * piece, piece)
        return w_all.at[pl.ds(first, count * piece)]

    def z_copy(d):
        return remote(
            w_out.at[pl.ds(pl.multiple_of(part * piece, piece), piece)],
            w_rows(0, part), z_send.at[d], z_recv.at[d], {"sp": lax.rem(sp + d, n_sp)},
        )

    def x_forward(d):
        at = w_rows(d, part)
        return remote(at, at, x_send.at[d], x_recv.at[d], {"tp": beside})

    def y_forward(d, second):
        at = w_rows(d, part_beside if second else part)
        k = 2 * d + second
        return remote(at, at, y_send.at[k], y_recv.at[k], {"grp": across})

    def c_forward(d):
        at = w_rows(d, core * n_grp * 2, n_grp * 2)
        return remote(at, at, c_send.at[d], c_recv.at[d], {"tp": mate})

    near = sorted({1, n_sp - 1})
    far = [d for d in range(2, n_sp - 1)]

    def forward_first(group):
        for d in group:
            z_copy(d).wait_recv()
            y_forward(d, 0).start()
            x_forward(d).start()

    def forward_second(group):
        for d in group:
            x_forward(d).wait_recv()
            y_forward(d, 1).start()

    def forward_third(group):
        for d in group:
            y_forward(d, 0).wait_recv()
            y_forward(d, 1).wait_recv()
            c_forward(d).start()

    def middle():
        forward_second(near)
        forward_first(far)

    head_last = heads - 1
    points = {(0, chunks - 3): lambda: forward_first(near)}
    points[(head_last, chunks - 2)] = lambda: forward_second(far)
    if heads == 1:
        points[(0, chunks - 2)] = middle
        points[(0, chunks - 1)] = lambda: forward_second(far)

    for d in near + far:
        z_copy(d).start()

    gain_row = in_gain[...]
    sublane = lax.broadcasted_iota(jnp.int32, (SUB // 8, 8, head), 1)

    def lanes_of(h):
        return slice(h * head, (h + 1) * head)

    def spread(row):
        return jnp.broadcast_to(row, (8, row.shape[1]))

    def start_conv(h):
        before = normalize(halo[...], gain_row)
        before = jnp.dot(before, wi[:, lanes_of(h)], preferred_element_type=F32)
        padded[0:8, :] = jnp.where(sp > 0, before[halo_rows - 8 :], 0.0)

    def phase_a(h, i, carry):
        lanes = lanes_of(h)
        at = pl.ds(pl.multiple_of(i * CHUNK, CHUNK), CHUNK)
        for (point_head, point), action in points.items():
            if point_head == h:
                pl.when(i == point)(action)
        if h == 0:
            x_copy(i).wait()
            x[at, :] = normalize(x[at, :], gain_row)
        normed = x[at, :]
        projected = jnp.dot(normed, wi[:, lanes], preferred_element_type=F32)
        padded[8:, :] = projected
        for r in range(0, CHUNK, SUB):
            summed = padded[8 - reach + r : 8 - reach + r + SUB, :] * taps[0:1, lanes]
            for k in range(1, reach + 1):
                first = 8 - reach + k + r
                summed = summed + padded[first : first + SUB, :] * taps[k : k + 1, lanes]
            conv[r : r + SUB, :] = summed.astype(BF16)
        padded[0:8, :] = padded[CHUNK:, :]
        rate_in[...] = jnp.dot(conv[...], halved[2 * h], preferred_element_type=F32)
        inlet_in[...] = jnp.dot(conv[...], halved[2 * h + 1], preferred_element_type=F32)
        gate_raw = jnp.dot(normed, wg[:, lanes], preferred_element_type=F32)
        gate[at, lanes] = gelu_half(gate_raw)
        bias_row = bias[h : h + 1, at] * (1.0 / math.log(2.0))
        bias_cols = jnp.broadcast_to(bias_row, (128, CHUNK)).T
        scale = rate_scale[0:1, lanes]
        s, p = carry
        for r in range(0, CHUNK, SUB):
            here = slice(r, r + SUB)
            into = pl.ds(pl.multiple_of(i * CHUNK + r, SUB), SUB)
            bias_here = jnp.concatenate([bias_cols[here]] * (head // 128), axis=1)
            log2_decay = jnp.tanh(rate_in[here, :]) * scale + (bias_here + scale)
            decay = jnp.exp2(log2_decay)
            left = one_minus_square(log2_decay, decay)
            drive = (
                left * lax.rsqrt(jnp.maximum(left, 1e-37))
                * ((1.0 + jnp.tanh(inlet_in[here, :])) * conv[here, :].astype(F32))
            )
            pt = decay.reshape(SUB // 8, 8, head)
            st = drive.reshape(SUB // 8, 8, head)
            for d in (1, 2, 4):
                inside = sublane >= d
                st = st + pt * jnp.where(inside, pltpu.roll(st, d, 1), 0.0)
                pt = pt * jnp.where(inside, pltpu.roll(pt, d, 1), 1.0)
            s_parts, p_parts = [], []
            for t in range(SUB // 8):
                s_parts.append(st[t] + pt[t] * s)
                p_parts.append(pt[t] * p)
                p_last = spread(pt[t, 7:8])
                s = spread(st[t, 7:8]) + p_last * s
                p = p_last * p
            state[into, lanes] = jnp.concatenate(s_parts, axis=0)
            prod[into, lanes] = jnp.concatenate(p_parts, axis=0)
        return s, p

    def start_carry():
        return jnp.zeros((8, head), F32), jnp.ones((8, head), F32)

    def end_copy(h, d):
        k = h * n_sp + d
        return remote(
            ends.at[h], ends_in.at[k], end_send.at[k], end_recv.at[k],
            {"sp": lax.rem(sp + d, n_sp)},
        )

    def send_ends(h, carry):
        s, p = carry
        ends[h, 0:8, :] = s
        ends[h, 8:16, :] = p
        for d in range(1, n_sp):
            end_copy(h, d).start()

    def take_ends(h):
        carry = jnp.zeros((8, head), F32)
        for d in range(n_sp - 1, 0, -1):
            end_copy(h, d).wait_recv()
            k = h * n_sp + d
            new = ends_in[k, 0:8, :] + ends_in[k, 8:16, :] * carry
            carry = jnp.where(d <= sp, new, carry)
        return carry[0:1]

    def a_copy(h, k):
        to = lax.rem(tp + k, n_tp)
        at = pl.ds(pl.multiple_of(to * out_rows, out_rows), out_rows)
        slot = h * n_tp + k
        return remote(
            gated.at[h, at], arrived.at[tp * heads + h], a_send.at[slot], a_recv.at[slot],
            {"tp": to},
        )

    def q_copy(h, k):
        to = lax.rem(tp + k, n_tp)
        slot = h * n_tp + k
        return remote(
            squares.at[h * n_tp + to], squares_in.at[tp * heads + h],
            q_send.at[slot], q_recv.at[slot], {"tp": to},
        )

    def own_copies(h):
        at = pl.ds(pl.multiple_of(tp * out_rows, out_rows), out_rows)
        return (
            pltpu.make_async_copy(gated.at[h, at], arrived.at[tp * heads + h], own_sem.at[2 * h]),
            pltpu.make_async_copy(
                squares.at[h * n_tp + tp], squares_in.at[tp * heads + h], own_sem.at[2 * h + 1]
            ),
        )

    order = list(range(2, n_tp)) + [1, 0]

    def phase_b(h, carry):
        lanes = lanes_of(h)
        for k in order:
            to = lax.rem(tp + k, n_tp)

            def block(j, _):
                sums = []
                for r in range(0, CHUNK, SUB):
                    first = j * CHUNK + r
                    at = pl.ds(pl.multiple_of(to * out_rows + first, SUB), SUB)
                    full = state[at, lanes] + prod[at, lanes] * carry
                    value = full * gate[at, lanes]
                    gated[h, at, :] = (value * out_gain[0:1, lanes]).astype(BF16)
                    square = value * value
                    part = square[:, 0:128]
                    for c in range(128, head, 128):
                        part = part + square[:, c : c + 128]
                    sums.append(part)
                row = jnp.sum(jnp.concatenate(sums, axis=0).T, axis=0, keepdims=True)
                squares[h * n_tp + to, :, pl.ds(pl.multiple_of(j * CHUNK, CHUNK), CHUNK)] = spread(row)
                return 0

            lax.fori_loop(0, out_rows // CHUNK, block, 0)
            if k == 0:
                for copy in own_copies(h):
                    copy.start()
            else:
                a_copy(h, k).start()
                q_copy(h, k).start()

    def wait_blocks(h):
        for copy in own_copies(h):
            copy.wait()
        for k in range(1, n_tp):
            a_copy(h, k).wait_recv()
            q_copy(h, k).wait_recv()

    def finish_w():
        for d in range(1, n_sp):
            c_forward(d).wait_recv()

    tile = 512 if width % 512 == 0 else 256

    def multiply(h, columns):
        left = jnp.concatenate([arrived[k * heads + h] for k in range(n_tp)], axis=1)
        right = jnp.concatenate(
            [w_all[(k * heads + h) * head : (k * heads + h + 1) * head, columns] for k in range(n_tp)],
            axis=0,
        )
        return jnp.dot(left, right, preferred_element_type=F32)

    for h in range(heads):
        halved[2 * h] = w_rate[h] * 0.5
        halved[2 * h + 1] = w_inlet[h] * 0.5

    loads[0].wait()
    carry = start_carry()
    halo_copy.wait_recv()
    start_conv(0)
    loads[1].wait()
    carry = lax.fori_loop(0, chunks, functools.partial(phase_a, 0), carry)
    send_ends(0, carry)
    split = min(2, chunks)
    for h in range(1, heads):
        start_conv(h)
        carry = lax.fori_loop(0, split, functools.partial(phase_a, h), start_carry())
        if h == 1:
            middle()
        phase_b(h - 1, take_ends(h - 1))
        carry = lax.fori_loop(split, chunks, functools.partial(phase_a, h), carry)
        send_ends(h, carry)
    last = heads - 1
    phase_b(last, take_ends(last))
    forward_third(near)
    forward_third(far)
    loads[2].wait()
    finish_w()
    for h in range(last):
        wait_blocks(h)

        def partial_sum(n, _, h=h):
            columns = pl.ds(pl.multiple_of(n * tile, tile), tile)
            value = multiply(h, columns)
            total[:, columns] = value if h == 0 else total[:, columns] + value
            return 0

        lax.fori_loop(0, width // tile, partial_sum, 0)
    wait_blocks(last)
    row = squares_in[0]
    for k in range(1, n_tp * heads):
        row = row + squares_in[k]
    out_scale = lax.rsqrt(row[0:1] / (n_tp * heads * head) + 1e-06)
    scale_cols = jnp.broadcast_to(out_scale, (128, out_rows)).T

    def out_copy(n):
        columns = pl.ds(pl.multiple_of(n * tile, tile), tile)
        return pltpu.make_async_copy(result.at[:, columns], out.at[:, columns], out_sem.at[n])

    def final(n, _):
        columns = pl.ds(pl.multiple_of(n * tile, tile), tile)
        value = multiply(last, columns)
        if last > 0:
            value = value + total[:, columns]
        value = value * jnp.concatenate([scale_cols] * (tile // 128), axis=1)
        result[:, columns] = value.astype(BF16)
        out_copy(n).start()
        return 0

    lax.fori_loop(0, width // tile, final, 0)

    halo_copy.wait_send()
    for d in range(1, n_sp):
        z_copy(d).wait_send()
        x_forward(d).wait_send()
        y_forward(d, 0).wait_send()
        y_forward(d, 1).wait_send()
        c_forward(d).wait_send()
        for h in range(heads):
            end_copy(h, d).wait_send()
    for h in range(heads):
        for k in range(1, n_tp):
            a_copy(h, k).wait_send()
            q_copy(h, k).wait_send()
    for n in range(width // tile):
        out_copy(n).wait()


def body(sizes, tokens, in_gain, w_input, w_gate, conv_taps, w_rate, w_inlet, decay_param,
         decay_bias, out_gain, w_out):
    n_grp, n_sp, n_tp = sizes
    rows, width = tokens.shape
    channels = w_input.shape[1]
    heads, head = w_rate.shape[0], w_rate.shape[1]
    out_rows = rows // n_tp
    out_width = w_out.shape[1]
    all_channels = channels * n_tp
    tile = 512 if out_width % 512 == 0 else 256
    rate_scale = (-4.0 / math.log(2.0) * jax.nn.softplus(-decay_param)).reshape(1, channels)
    hbm = pl.BlockSpec(memory_space=pl.ANY)
    vmem = pl.BlockSpec(memory_space=pltpu.VMEM)
    dma = pltpu.SemaphoreType.DMA
    return pl.pallas_call(
        functools.partial(kernel, sizes),
        out_shape=jax.ShapeDtypeStruct((out_rows, out_width), BF16),
        in_specs=[hbm, vmem, hbm, hbm, vmem, vmem, vmem, vmem, vmem, vmem, hbm],
        out_specs=hbm,
        scratch_shapes=[
            pltpu.VMEM((rows, width), BF16),
            pltpu.VMEM((width, channels), BF16),
            pltpu.VMEM((width, channels), BF16),
            pltpu.VMEM((all_channels, out_width), BF16),
            pltpu.VMEM((rows, channels), F32),
            pltpu.VMEM((rows, channels), F32),
            pltpu.VMEM((rows, channels), F32),
            pltpu.VMEM((heads, rows, head), BF16),
            pltpu.VMEM((n_tp * heads, out_rows, head), BF16),
            pltpu.VMEM((out_rows, out_width), F32),
            pltpu.VMEM((out_rows, out_width), BF16),
            pltpu.VMEM((16, width), BF16),
            pltpu.VMEM((CHUNK + 8, head), F32),
            pltpu.VMEM((CHUNK, head), BF16),
            pltpu.VMEM((2 * heads, head, head), BF16),
            pltpu.VMEM((CHUNK, head), F32),
            pltpu.VMEM((CHUNK, head), F32),
            pltpu.VMEM((heads * n_tp, 8, out_rows), F32),
            pltpu.VMEM((n_tp * heads, 8, out_rows), F32),
            pltpu.VMEM((heads, 16, head), F32),
            pltpu.VMEM((heads * n_sp, 16, head), F32),
            dma((rows // CHUNK,)),
            dma((3,)),
            dma,
            dma,
            dma((n_sp,)),
            dma((n_sp,)),
            dma((n_sp,)),
            dma((n_sp,)),
            dma((2 * n_sp,)),
            dma((2 * n_sp,)),
            dma((n_sp,)),
            dma((n_sp,)),
            dma((heads * n_sp,)),
            dma((heads * n_sp,)),
            dma((heads * n_tp,)),
            dma((heads * n_tp,)),
            dma((heads * n_tp,)),
            dma((heads * n_tp,)),
            dma((2 * heads,)),
            dma((out_width // tile,)),
        ],
        compiler_params=pltpu.CompilerParams(
            collective_id=0, has_side_effects=True, vmem_limit_bytes=62 * 1024 * 1024
        ),
    )(
        tokens, in_gain.reshape(1, width), w_input, w_gate, conv_taps, w_rate, w_inlet,
        rate_scale, decay_bias, out_gain.reshape(1, channels), w_out,
    )


def solution(mesh):
    sizes = (mesh.shape["grp"], mesh.shape["sp"], mesh.shape["tp"])
    return jax.shard_map(
        functools.partial(body, sizes),
        mesh=mesh,
        in_specs=(
            P(("grp", "sp"), None),
            P(),
            P(None, "tp"),
            P(None, "tp"),
            P(None, "tp"),
            P("tp", None, None),
            P("tp", None, None),
            P("tp"),
            P("tp", ("grp", "sp")),
            P("tp"),
            P("sp", None),
        ),
        out_specs=P(("grp", "sp", "tp"), None),
        check_vma=False,
    )
```

profile of v0, /device:TPU:1, one launch (start us, length us, event | category | flops | bytes accessed | tf_op | source)
XLA Modules:
  0.0 72.9 jit_solution(7451272660544766616)
XLA Ops:
  0.0 1.3 %fusion = f32[512]{0:T(512)} fusion(f32[512]{0:T(512)} %param.18), kind=kLoop, calls=%fused_computation.1 | loop fusion | flops 4096 | bytes 4096 | tf_op jit(solution)/shard_map/mul | solution.py:427
  1.3 68.4 %shard_map.109 = bf16[512,2048]{1,0:T(8,128)(2,1)} custom-call(bf16[2048,2048]{1,0:T(8,128)(2,1)} %tokens.1, f32[1,2048]{1,0:T(1,128)} %bitcast.3, bf16[2048,512]{1,0:T(8,128)(2,1)} %w_input.1, bf16[2048,512]{1,0:T(8,128)(2,1)} %w_gate.1, f32[4,512]{1,0:T(4,128)} %taps.1, bf16[2,256,256]{2,1,0:T(8,128)(2,1)} %w_rate.1, bf16[2,256,256]{2,1,0:T(8,128)(2,1)} %w_inlet.1, ...), custom_call_target="tpu_custom_call" | custom-call | tf_op jit(solution)/shard_map/pallas_call | solution.py:431
  69.7 3.2 %copy.13 = bf16[512,2048]{1,0:T(8,128)(2,1)} copy(bf16[512,2048]{1,0:T(8,128)(2,1)} %shard_map.109) | data formatting | bytes 4194304
where the time goes:
time: 73.1 us; the launch traced here: 72.9 us
  Pallas kernels  68.4 us (94%)
  local copies, waits for them, and re-layouts  3.16 us (4%)
  other arithmetic  1.28 us (2%)
    pallas_call x1, Pallas kernels, body(): pl.pallas_call(functools.partial(kernel, sizes), out_shape=jax.ShapeDtype...  68.4 us
    unnamed x1, local copies, waits for them, and re-layouts  3.16 us

commit v1 on v0

v1 whole, which is shorter than its diff:
```python
import functools
import math
import jax
import jax.numpy as jnp
from jax import lax
from jax.experimental import pallas as pl
from jax.experimental.pallas import tpu as pltpu
from jax.sharding import PartitionSpec as P

MESH = pl.DeviceIdType.MESH
F32 = jnp.float32
BF16 = jnp.bfloat16
CHUNK = 256
SEG = CHUNK // 8
STRIDE = SEG + 8
LANES = 128
LAG = 2
FIRST = 3
EVERY = 3
BEHIND = 4
AHEAD = 6
BETWEEN = 1
LN2 = math.log(2.0)
GELU_A = math.sqrt(2.0 / math.pi)
GELU_B = GELU_A * 0.044715


def gelu_half(value):
    inner = value * (GELU_A + GELU_B * (value * value))
    return (0.25 * value) * (1.0 + jnp.tanh(inner))


def softplus_of_minus(value):
    small = jnp.exp(-jnp.abs(value))
    z = small / (2.0 + small)
    zz = z * z
    series = 1.0 / 15.0
    for n in (13, 11, 9, 7, 5, 3, 1):
        series = series * zz + 1.0 / n
    return jnp.maximum(-value, 0.0) + 2.0 * z * series


def spread(row):
    return jnp.broadcast_to(row, (8, row.shape[1]))


def columns_of(row):
    return jnp.broadcast_to(row, (LANES, row.shape[1])).T


def kernel(
    sizes,
    tokens, in_gain, w_input, w_gate, taps, w_rate, w_inlet, decay_param, bias, out_gain, w_out,
    out,
    x, w_in, w_all, gates_w, inv, proj, graw, conv, raw, bias_p, scale_row, before,
    state, prod, gate, pre_s, pre_p, natural, gated, arrived, total, result, halo,
    squares, squares_in, ends, ends_in,
    x_sem, w_sem, out_load_sem, halo_send, halo_recv, z_send, z_recv, y_send, y_recv,
    m_send, m_recv, end_send, end_recv, a_send, a_recv, q_send, q_recv, own_sem, out_sem,
):
    n_grp, n_sp, n_tp = sizes
    grp, sp, tp = lax.axis_index("grp"), lax.axis_index("sp"), lax.axis_index("tp")
    rows, width = tokens.shape
    heads, head = w_rate.shape[0], w_rate.shape[1]
    parts = head // LANES
    channels = heads * head
    reach = taps.shape[0] - 1
    chunks = rows // CHUNK
    steps = heads * chunks
    out_rows = rows // n_tp
    per_owner = out_rows // CHUNK
    shard = w_out.shape[0]
    quarter = shard // (2 * n_grp)
    piece = max(16, quarter // 4)
    pieces = quarter // piece
    items = (n_sp - 1) * pieces
    core = lax.rem(tp, 2)
    mate = tp + 1 - 2 * core
    across = 1 - grp

    def x_copy(i):
        at = pl.ds(pl.multiple_of(i * CHUNK, CHUNK), CHUNK)
        return pltpu.make_async_copy(tokens.at[at], x.at[at], x_sem.at[i])

    def w_copies(h):
        lanes = pl.ds(h * head, head)
        return (
            pltpu.make_async_copy(w_input.at[:, lanes], w_in.at[h, :, 0:head], w_sem.at[2 * h]),
            pltpu.make_async_copy(
                w_gate.at[:, lanes], w_in.at[h, :, head : 2 * head], w_sem.at[2 * h + 1]
            ),
        )

    out_load = pltpu.make_async_copy(
        w_out, w_all.at[pl.ds(pl.multiple_of(sp * shard, shard), shard)], out_load_sem
    )

    ends_in[...] = jnp.zeros_like(ends_in)
    barrier = pltpu.get_barrier_semaphore()
    for d in range(1, n_sp):
        pl.semaphore_signal(
            barrier, inc=1, device_id={"sp": lax.rem(sp + d, n_sp)}, device_id_type=MESH
        )
    for k in range(1, n_tp):
        pl.semaphore_signal(
            barrier, inc=1, device_id={"tp": lax.rem(tp + k, n_tp)}, device_id_type=MESH
        )
    pl.semaphore_signal(barrier, inc=1, device_id={"grp": across}, device_id_type=MESH)

    for copy in w_copies(0):
        copy.start()
    x_copy(0).start()

    def remote(src, dst, send, recv, where):
        return pltpu.make_async_remote_copy(
            src_ref=src, dst_ref=dst, send_sem=send, recv_sem=recv,
            device_id=where, device_id_type=MESH,
        )

    halo_rows = halo.shape[0]
    halo_copy = remote(
        tokens.at[pl.ds(rows - halo_rows, halo_rows)], halo, halo_send, halo_recv,
        {"sp": jnp.minimum(sp + 1, n_sp - 1)},
    )

    def w_rows(source, which, p):
        first = source * shard + which * quarter + p * piece
        return w_all.at[pl.ds(pl.multiple_of(first, piece), piece)]

    def which_of(other, owner):
        return (across if other else grp) * 2 + owner

    def own_copy(to_right, p):
        mine = which_of(False, core)
        first = pl.multiple_of(mine * quarter + p * piece, piece)
        slot = ((0 if to_right else 1) * n_sp + sp) * pieces + p
        return remote(
            w_out.at[pl.ds(first, piece)], w_rows(sp, mine, p),
            z_send.at[slot], z_recv.at[sp * pieces + p],
            {"sp": jnp.minimum(sp + 1, n_sp - 1) if to_right else jnp.maximum(sp - 1, 0)},
        )

    def z_copy(source, p, to_right):
        at = w_rows(source, which_of(False, core), p)
        slot = ((0 if to_right else 1) * n_sp + source) * pieces + p
        return remote(
            at, at, z_send.at[slot], z_recv.at[source * pieces + p],
            {"sp": jnp.minimum(sp + 1, n_sp - 1) if to_right else jnp.maximum(sp - 1, 0)},
        )

    def y_copy(source, p, incoming=False):
        at = w_rows(source, which_of(incoming, core), p)
        slot = source * pieces + p
        return remote(at, at, y_send.at[slot], y_recv.at[slot], {"grp": across})

    def m_copy(source, p, second, incoming=False):
        at = w_rows(source, which_of(second, 1 - core if incoming else core), p)
        slot = ((1 if second else 0) * n_sp + source) * pieces + p
        return remote(at, at, m_send.at[slot], m_recv.at[slot], {"tp": mate})

    inner = jnp.minimum(sp, n_sp - 1 - sp)
    leftward = sp > n_sp - 1 - sp

    def source_of(b):
        d = jnp.where(b <= 2 * inner, (b + 1) // 2, b - inner)
        from_left = jnp.where(b <= 2 * inner, b % 2 == 1, leftward)
        return jnp.where(from_left, sp - d, sp + d)

    held = 2

    def each_source(n, action):
        d, p = 1 + n // pieces, n % pieces

        @pl.when(sp >= d)
        def _():
            action(sp - d, p, True)

        @pl.when(sp + d < n_sp)
        def _():
            action(sp + d, p, False)

    def onward(source, p, from_left, act):
        if from_left:
            pl.when(sp < n_sp - 1)(lambda: act(z_copy(source, p, True)))
        else:
            pl.when(sp > 0)(lambda: act(z_copy(source, p, False)))

    def take_z(source, p, from_left):
        z_copy(source, p, from_left).wait_recv()
        y_copy(source, p).start()
        m_copy(source, p, False).start()

    def take_y(source, p, from_left):
        y_copy(source, p, True).wait_recv()
        m_copy(source, p, True).start()

    def send_on(up, source, p, from_left):
        if up == from_left:
            onward(source, p, from_left, lambda copy: copy.start())

    def pump(n):
        @pl.when(n < items)
        def _():
            each_source(n, take_z)
            each_source(n, functools.partial(send_on, False))

        @pl.when((n >= held) & (n < items))
        def _():
            each_source(n, functools.partial(send_on, True))

        @pl.when(n == held)
        def _():
            for k in range(held):
                each_source(k, functools.partial(send_on, True))

        @pl.when(n >= LAG)
        def _():
            each_source(n - LAG, take_y)

    def fold(h):
        for copy in w_copies(h):
            copy.wait()

        def block(j, _):
            at = pl.ds(pl.multiple_of(j * CHUNK, CHUNK), CHUNK)
            gain = columns_of(in_gain[0:1, at])
            for c in range(2 * parts):
                lanes = slice(c * LANES, (c + 1) * LANES)
                w_in[h, at, lanes] = (w_in[h, at, lanes].astype(F32) * gain).astype(BF16)
            return 0

        lax.fori_loop(0, width // CHUNK, block, 0)

    def norm_of(chunk):
        as_float = chunk.astype(F32)
        return lax.rsqrt(jnp.mean(as_float * as_float, axis=1, keepdims=True) + 1e-06)

    def lanes_of(h, c):
        return pl.ds(pl.multiple_of(h * head + c * LANES, LANES), LANES)

    def project(s, sums):
        h, i = s // chunks, s % chunks
        at = pl.ds(pl.multiple_of(i * CHUNK, CHUNK), CHUNK)
        acc = jnp.dot(x[at, :], w_in[h], preferred_element_type=F32)
        if sums:
            scale = jnp.broadcast_to(norm_of(x[at, :]), (CHUNK, LANES))
            inv[at, :] = scale
        else:
            scale = inv[at, :]
        return acc, scale

    def keep(s, acc, scale):
        h, i = s // chunks, s % chunks
        for c in range(parts):
            last = proj[c, 7 * STRIDE + SEG : 8 * STRIDE, :]
            proj[c, 0:8, :] = jnp.where(i == 0, before[h, c], last)
            for g in range(8):
                at = slice(g * SEG, (g + 1) * SEG)
                block = acc[at, c * LANES : (c + 1) * LANES] * scale[at]
                proj[c, g * STRIDE + 8 : (g + 1) * STRIDE, :] = block
                if g < 7:
                    proj[c, (g + 1) * STRIDE : (g + 1) * STRIDE + 8, :] = block[SEG - 8 :]
                other = acc[at, head + c * LANES : head + (c + 1) * LANES] * scale[at]
                graw[c, g * STRIDE : g * STRIDE + SEG, :] = other

    def convolve(s):
        h, i = s // chunks, s % chunks
        for c in range(parts):
            lanes = lanes_of(h, c)
            tap = [spread(taps[k : k + 1, lanes]) for k in range(reach + 1)]
            window = [
                proj[c, pl.ds(8 - reach + j, 8, stride=STRIDE), :] for j in range(SEG + reach)
            ]
            done = []
            for k in range(SEG):
                summed = window[k] * tap[0]
                for j in range(1, reach + 1):
                    summed = summed + window[k + j] * tap[j]
                done.append(summed)
            for k in range(SEG):
                value = graw[c, pl.ds(k, 8, stride=STRIDE), :]
                gate[s, c, k * 8 : k * 8 + 8, :] = gelu_half(value)
            for k in range(0, SEG, 2):
                pair = jnp.concatenate(done[k : k + 2], axis=0).astype(BF16)
                conv[k * 8 : k * 8 + 16, c * LANES : (c + 1) * LANES] = pair
        row = bias[pl.ds(h, 1), pl.ds(pl.multiple_of(i * CHUNK, CHUNK), CHUNK)] * (1.0 / LN2)
        cols = columns_of(row)
        for g in range(8):
            bias_p[g * STRIDE : g * STRIDE + SEG, :] = cols[g * SEG : (g + 1) * SEG]
        raw[...] = jnp.dot(conv[...], gates_w[h], preferred_element_type=F32)

    sublane = lax.broadcasted_iota(jnp.int32, (8, LANES), 0)

    def elementwise(s, carry):
        h, i = s // chunks, s % chunks
        after = []
        for c in range(parts):
            scale = spread(scale_row[0:1, lanes_of(h, c)])
            lanes = slice(c * LANES, (c + 1) * LANES)
            st, pt = jnp.zeros((8, LANES), F32), jnp.ones((8, LANES), F32)
            for k in range(SEG):
                at = slice(k * 8, k * 8 + 8)
                if k % 2 == 0:
                    pair = conv[k * 8 : k * 8 + 16, lanes].astype(F32)
                value = pair[(k % 2) * 8 : (k % 2) * 8 + 8]
                shift = bias_p[pl.ds(k, 8, stride=STRIDE), :] + scale
                log2_decay = jnp.tanh(raw[at, lanes]) * scale + shift
                decay = jnp.exp2(log2_decay)
                left = jnp.tanh(log2_decay * -LN2) * (1.0 + decay * decay)
                inlet = raw[at, head + c * LANES : head + (c + 1) * LANES]
                drive = (
                    left * lax.rsqrt(jnp.maximum(left, 1e-37)) * ((1.0 + jnp.tanh(inlet)) * value)
                )
                st = decay * st + drive
                pt = decay * pt
                state[s, c, at, :] = st
                prod[s, c, at, :] = pt
            for d in (1, 2, 4):
                inside = sublane >= d
                st = st + pt * jnp.where(inside, pltpu.roll(st, d, 0), 0.0)
                pt = pt * jnp.where(inside, pltpu.roll(pt, d, 0), 1.0)
            s_in = jnp.where(i == 0, 0.0, carry[2 * c])
            p_in = jnp.where(i == 0, 1.0, carry[2 * c + 1])
            inside = sublane >= 1
            s_ex = jnp.where(inside, pltpu.roll(st, 1, 0), 0.0)
            p_ex = jnp.where(inside, pltpu.roll(pt, 1, 0), 1.0)
            pre_s[s, c] = s_ex + p_ex * s_in
            pre_p[s, c] = p_ex * p_in
            p_last = spread(pt[7:8])
            after += [spread(st[7:8]) + p_last * s_in, p_last * p_in]
        return tuple(after)

    def start_carry():
        zero, one = jnp.zeros((8, LANES), F32), jnp.ones((8, LANES), F32)
        return (zero, one) * parts

    def end_copy(h, d):
        k = h * n_sp + d
        return remote(
            ends.at[h], ends_in.at[k], end_send.at[k], end_recv.at[k],
            {"sp": jnp.minimum(sp + d, n_sp - 1)},
        )

    def send_ends(h, carry):
        for c in range(parts):
            ends[h, c, 0:8, :] = carry[2 * c]
            ends[h, c, 8:16, :] = carry[2 * c + 1]
        for d in range(1, n_sp):
            pl.when(sp + d < n_sp)(end_copy(h, d).start)

    def take_ends(h):
        carry = [jnp.zeros((8, LANES), F32)] * parts
        for d in range(n_sp - 1, 0, -1):
            pl.when(sp >= d)(end_copy(h, d).wait_recv)
            k = h * n_sp + d
            for c in range(parts):
                new = ends_in[k, c, 0:8, :] + ends_in[k, c, 8:16, :] * carry[c]
                carry[c] = jnp.where(d <= sp, new, carry[c])
        return carry

    def a_copy(h, k):
        to = lax.rem(tp + k, n_tp)
        at = pl.ds(pl.multiple_of(to * out_rows, out_rows), out_rows)
        slot = h * n_tp + k
        return remote(
            gated.at[h, at], arrived.at[tp * heads + h], a_send.at[slot], a_recv.at[slot],
            {"tp": to},
        )

    def q_copy(h, k):
        to = lax.rem(tp + k, n_tp)
        slot = h * n_tp + k
        return remote(
            squares.at[h * n_tp + to], squares_in.at[tp * heads + h],
            q_send.at[slot], q_recv.at[slot], {"tp": to},
        )

    def own_copies(h):
        at = pl.ds(pl.multiple_of(tp * out_rows, out_rows), out_rows)
        return (
            pltpu.make_async_copy(gated.at[h, at], arrived.at[tp * heads + h], own_sem.at[2 * h]),
            pltpu.make_async_copy(
                squares.at[h * n_tp + tp], squares_in.at[tp * heads + h], own_sem.at[2 * h + 1]
            ),
        )

    order = list(range(2, n_tp)) + [1, 0]

    def phase_b(h, carry):
        gains = [spread(out_gain[0:1, lanes_of(h, c)]) for c in range(parts)]

        def block(to, j):
            s = h * chunks + to * per_owner + j
            for c in range(parts):
                start = pre_s[s, c] + pre_p[s, c] * carry[c]
                for k in range(SEG):
                    at = slice(k * 8, k * 8 + 8)
                    full = state[s, c, at, :] + prod[s, c, at, :] * start
                    natural[c, pl.ds(k, 8, stride=STRIDE), :] = full * gate[s, c, at, :]
            first = pl.multiple_of(to * out_rows + j * CHUNK, CHUNK)
            sums = []
            for g in range(8):
                part = None
                for c in range(parts):
                    value = natural[c, g * STRIDE : g * STRIDE + SEG, :]
                    gain = jnp.concatenate([gains[c]] * (SEG // 8), axis=0)
                    into = pl.ds(pl.multiple_of(first + g * SEG, SEG), SEG)
                    gated[h, into, c * LANES : (c + 1) * LANES] = (value * gain).astype(BF16)
                    part = value * value if part is None else part + value * value
                sums.append(part)
            row = jnp.sum(jnp.concatenate(sums, axis=0).T, axis=0, keepdims=True)
            at = pl.ds(pl.multiple_of(j * CHUNK, CHUNK), CHUNK)
            squares[h * n_tp + to, :, at] = spread(row)

        def owner(n, _):
            k = lax.rem(n + 2, n_tp)
            k = jnp.where(n == n_tp - 2, 1, jnp.where(n == n_tp - 1, 0, k))
            to = lax.rem(tp + k, n_tp)

            def one(j, _):
                block(to, j)
                return 0

            lax.fori_loop(0, per_owner, one, 0)

            @pl.when(k == 0)
            def _():
                for copy in own_copies(h):
                    copy.start()

            @pl.when(k > 0)
            def _():
                a_copy(h, k).start()
                q_copy(h, k).start()

            return 0

        lax.fori_loop(0, n_tp, owner, 0)

    h_all = range(heads)
    for h in h_all:
        gates_w[h, :, 0:head] = w_rate[h] * 0.5
        gates_w[h, :, head : 2 * head] = w_inlet[h] * 0.5
    scale_row[...] = softplus_of_minus(decay_param[...]) * (-4.0 / LN2)
    fold(0)
    x_copy(0).wait()
    x_copy(1).start()
    for h in range(1, heads):
        for copy in w_copies(h):
            copy.start()
    acc, scale = project(0, True)
    for c in range(parts):
        proj[c, 7 * STRIDE + SEG : 8 * STRIDE, :] = jnp.zeros((8, LANES), F32)

    pl.semaphore_wait(barrier, n_sp - 1 + n_tp - 1 + 1)
    pl.when(sp < n_sp - 1)(halo_copy.start)
    for p in range(pieces):
        pl.when(sp < n_sp - 1)(own_copy(True, p).start)
        pl.when(sp > 0)(own_copy(False, p).start)
    for h in range(1, heads):
        fold(h)
    for i in range(2, chunks):
        x_copy(i).start()
    out_load.start()

    @pl.when(sp == 0)
    def _():
        before[...] = jnp.zeros_like(before)

    @pl.when(sp > 0)
    def _():
        halo_copy.wait_recv()
        halo_inv = norm_of(halo[...])
        for h in h_all:
            rows_before = jnp.dot(halo[...], w_in[h, :, 0:head], preferred_element_type=F32)
            rows_before = rows_before * halo_inv
            for c in range(parts):
                before[h, c] = rows_before[halo_rows - 8 :, c * LANES : (c + 1) * LANES]

    keep(0, acc, scale)
    x_copy(1).wait()
    acc, scale = project(1, True)
    convolve(0)
    keep(1, acc, scale)

    def finish_step(s, carry):
        @pl.when(s % chunks == chunks - 1)
        def _():
            send_ends(s // chunks, carry)

    def step(sums, s, carry):
        if sums:
            x_copy(s + 2).wait()

        @pl.when((s >= FIRST) & ((s - FIRST) % EVERY == 0))
        def _():
            pump((s - FIRST) // EVERY)

        if not sums and heads > 1:

            @pl.when((s >= chunks) & (s % chunks == BEHIND))
            def _():
                phase_b(s // chunks - 1, take_ends(s // chunks - 1))

        acc, scale = project(s + 2, sums)
        carry = elementwise(s, carry)
        convolve(s + 1)
        keep(s + 2, acc, scale)
        finish_step(s, carry)
        return carry

    carry = start_carry()
    carry = lax.fori_loop(0, chunks - 2, functools.partial(step, True), carry)
    carry = lax.fori_loop(chunks - 2, steps - 2, functools.partial(step, False), carry)
    done = -((FIRST - steps + 2) // EVERY)
    carry = elementwise(steps - 2, carry)
    convolve(steps - 1)
    carry = elementwise(steps - 1, carry)
    last = heads - 1
    send_ends(last, carry)
    pump(done)
    done += 1

    def pump_some(first, end):
        def one(n, _):
            pump(n)
            return 0

        lax.fori_loop(first, end, one, 0)

    phase_b(last, take_ends(last))
    out_load.wait()

    progressive = shard == channels
    tile = 512 if width % 512 == 0 else 256
    deep = min(shard, head)

    def wait_from(k, h):
        @pl.when(k == 0)
        def _():
            for copy in own_copies(h):
                copy.wait()

        @pl.when(k > 0)
        def _():
            a_copy(h, k).wait_recv()
            q_copy(h, k).wait_recv()

    def wait_mate(b):
        source = source_of(b)

        def one(p, _):
            m_copy(source, p, False, True).wait_recv()
            m_copy(source, p, True, True).wait_recv()
            return 0

        lax.fori_loop(0, pieces, one, 0)

    def prepare(b, h):
        source = source_of(b)
        if progressive:
            wait_from(lax.rem(tp - source + n_tp, n_tp), h)
        return source

    def multiply(source, columns, units):
        blocks = []
        for u in units:
            at = source * shard + u * deep
            from_col = pl.multiple_of(at % head, deep)
            blocks.append(arrived[at // head, :, pl.ds(from_col, deep)])
        left = jnp.concatenate(blocks, axis=1)
        first = pl.multiple_of(source * shard + units[0] * deep, deep)
        right = w_all[pl.ds(first, len(units) * deep), columns]
        return jnp.dot(left, right, preferred_element_type=F32)

    def columns_at(n):
        return pl.ds(pl.multiple_of(n * tile, tile), tile)

    if not progressive:
        for k in range(n_tp):
            for h in h_all:
                wait_from(k, h)
    units = shard // deep
    work = [(b, u) for u in range(units) for b in range(n_sp - 1)]
    ahead = max(done, AHEAD * items // 12)
    pump_some(done, ahead)
    cursor = ahead
    mates = {0}
    for index, (b, u) in enumerate(work):
        needed = b * pieces + LAG
        if index >= n_sp - 1 and progressive:
            needed = items + LAG
        if b > 0:
            pump_some(cursor, max(cursor, needed))
            cursor = max(cursor, needed)
        if b not in mates:
            wait_mate(b)
            mates.add(b)
        source = prepare(b, u)

        def partial_sum(n, _, source=source, index=index, u=u, cursor=cursor):
            columns = columns_at(n)
            value = multiply(source, columns, (u,))
            total[:, columns] = value if index == 0 else total[:, columns] + value

            @pl.when((n < BETWEEN) & (cursor + n < items + LAG))
            def _():
                pump(cursor + n)

            return 0

        lax.fori_loop(0, width // tile, partial_sum, 0)
        cursor = min(cursor + BETWEEN, items + LAG)
    b = n_sp - 1
    if b > 0:
        pump_some(cursor, items + LAG)
        wait_mate(b)
    for u in range(units):
        source = prepare(b, u)
    row = squares_in[0]
    for k in range(1, n_tp * heads):
        row = row + squares_in[k]
    out_scale = lax.rsqrt(row[0:1] / (n_tp * heads * head) + 1e-06)
    scale_cols = jnp.broadcast_to(out_scale, (LANES, out_rows)).T

    def out_copy(n):
        columns = columns_at(n)
        return pltpu.make_async_copy(result.at[:, columns], out.at[:, columns], out_sem.at[n])

    def final(n, _):
        columns = columns_at(n)
        value = multiply(source, columns, tuple(range(units)))
        if n_sp > 1:
            value = value + total[:, columns]
        value = value * jnp.concatenate([scale_cols] * (tile // LANES), axis=1)
        result[:, columns] = value.astype(BF16)
        out_copy(n).start()
        return 0

    lax.fori_loop(0, width // tile, final, 0)

    pl.when(sp < n_sp - 1)(halo_copy.wait_send)
    for p in range(pieces):
        pl.when(sp < n_sp - 1)(own_copy(True, p).wait_send)
        pl.when(sp > 0)(own_copy(False, p).wait_send)

    def drain_one(source, p, from_left):
        onward(source, p, from_left, lambda copy: copy.wait_send())
        y_copy(source, p).wait_send()
        m_copy(source, p, False).wait_send()
        m_copy(source, p, True).wait_send()

    def drain(n, _):
        each_source(n, drain_one)
        return 0

    lax.fori_loop(0, items, drain, 0)
    for h in h_all:
        for d in range(1, n_sp):
            pl.when(sp + d < n_sp)(end_copy(h, d).wait_send)
        for k in range(1, n_tp):
            a_copy(h, k).wait_send()
            q_copy(h, k).wait_send()
    for n in range(width // tile):
        out_copy(n).wait()


def body(sizes, tokens, in_gain, w_input, w_gate, conv_taps, w_rate, w_inlet, decay_param,
         decay_bias, out_gain, w_out):
    n_grp, n_sp, n_tp = sizes
    rows, width = tokens.shape
    channels = w_input.shape[1]
    heads, head = w_rate.shape[0], w_rate.shape[1]
    parts = head // LANES
    steps = heads * (rows // CHUNK)
    out_rows = rows // n_tp
    out_width = w_out.shape[1]
    shard = w_out.shape[0]
    quarter = shard // (2 * n_grp)
    pieces = quarter // max(16, quarter // 4)
    all_channels = channels * n_tp
    tile = 512 if out_width % 512 == 0 else 256
    hbm = pl.BlockSpec(memory_space=pl.ANY)
    vmem = pl.BlockSpec(memory_space=pltpu.VMEM)
    dma = pltpu.SemaphoreType.DMA
    return pl.pallas_call(
        functools.partial(kernel, sizes),
        out_shape=jax.ShapeDtypeStruct((out_rows, out_width), BF16),
        in_specs=[hbm, vmem, hbm, hbm, vmem, vmem, vmem, vmem, vmem, vmem, hbm],
        out_specs=hbm,
        scratch_shapes=[
            pltpu.VMEM((rows, width), BF16),
            pltpu.VMEM((heads, width, 2 * head), BF16),
            pltpu.VMEM((all_channels, out_width), BF16),
            pltpu.VMEM((heads, head, 2 * head), BF16),
            pltpu.VMEM((rows, LANES), F32),
            pltpu.VMEM((parts, 8 * STRIDE, LANES), F32),
            pltpu.VMEM((parts, 8 * STRIDE, LANES), F32),
            pltpu.VMEM((CHUNK, head), BF16),
            pltpu.VMEM((CHUNK, 2 * head), F32),
            pltpu.VMEM((8 * STRIDE, LANES), F32),
            pltpu.VMEM((1, channels), F32),
            pltpu.VMEM((heads, parts, 8, LANES), F32),
            pltpu.VMEM((steps, parts, CHUNK, LANES), F32),
            pltpu.VMEM((steps, parts, CHUNK, LANES), F32),
            pltpu.VMEM((steps, parts, CHUNK, LANES), F32),
            pltpu.VMEM((steps, parts, 8, LANES), F32),
            pltpu.VMEM((steps, parts, 8, LANES), F32),
            pltpu.VMEM((parts, 8 * STRIDE, LANES), F32),
            pltpu.VMEM((heads, rows, head), BF16),
            pltpu.VMEM((n_tp * heads, out_rows, head), BF16),
            pltpu.VMEM((out_rows, out_width), F32),
            pltpu.VMEM((out_rows, out_width), BF16),
            pltpu.VMEM((16, width), BF16),
            pltpu.VMEM((heads * n_tp, 8, out_rows), F32),
            pltpu.VMEM((n_tp * heads, 8, out_rows), F32),
            pltpu.VMEM((heads, parts, 16, LANES), F32),
            pltpu.VMEM((heads * n_sp, parts, 16, LANES), F32),
            dma((rows // CHUNK,)),
            dma((2 * heads,)),
            dma,
            dma,
            dma,
            dma((2 * n_sp * pieces,)),
            dma((n_sp * pieces,)),
            dma((n_sp * pieces,)),
            dma((n_sp * pieces,)),
            dma((2 * n_sp * pieces,)),
            dma((2 * n_sp * pieces,)),
            dma((heads * n_sp,)),
            dma((heads * n_sp,)),
            dma((heads * n_tp,)),
            dma((heads * n_tp,)),
            dma((heads * n_tp,)),
            dma((heads * n_tp,)),
            dma((2 * heads,)),
            dma((out_width // tile,)),
        ],
        compiler_params=pltpu.CompilerParams(
            collective_id=0, has_side_effects=True, vmem_limit_bytes=62 * 1024 * 1024
        ),
    )(
        tokens, in_gain.reshape(1, width), w_input, w_gate, conv_taps, w_rate, w_inlet,
        decay_param.reshape(1, channels), decay_bias, out_gain.reshape(1, channels), w_out,
    )


def solution(mesh):
    sizes = (mesh.shape["grp"], mesh.shape["sp"], mesh.shape["tp"])
    return jax.shard_map(
        functools.partial(body, sizes),
        mesh=mesh,
        in_specs=(
            P(("grp", "sp"), None),
            P(),
            P(None, "tp"),
            P(None, "tp"),
            P(None, "tp"),
            P("tp", None, None),
            P("tp", None, None),
            P("tp"),
            P("tp", ("grp", "sp")),
            P("tp"),
            P("sp", None),
        ),
        out_specs=P(("grp", "sp", "tp"), None),
        check_vma=False,
    )
```

time: 73.1 us -> 65.1 us (0.89)
  the two profiles are of different devices: /device:TPU:1 before, /device:TPU:24 now
where the time goes in v1:
time: 65.1 us; the launch traced here: 64.9 us
  Pallas kernels  61.7 us (95%)
  local copies, waits for them, and re-layouts  3.16 us (5%)
    pallas_call x1, Pallas kernels, body(): pl.pallas_call(functools.partial(kernel, sizes), out_shape=jax.ShapeDtype...  61.7 us
    unnamed x1, local copies, waits for them, and re-layouts  3.16 us

profile of v1, /device:TPU:24, one launch (start us, length us, event | category | flops | bytes accessed | tf_op | source)
XLA Modules:
  0.0 64.9 jit_solution(9725499014404311207)
XLA Ops:
  0.0 61.7 %shard_map.109 = bf16[512,2048]{1,0:T(8,128)(2,1)} custom-call(bf16[2048,2048]{1,0:T(8,128)(2,1)} %tokens.1, f32[1,2048]{1,0:T(1,128)} %bitcast.3, bf16[2048,512]{1,0:T(8,128)(2,1)} %w_input.1, bf16[2048,512]{1,0:T(8,128)(2,1)} %w_gate.1, f32[4,512]{1,0:T(4,128)} %taps.1, bf16[2,256,256]{2,1,0:T(8,128)(2,1)} %w_rate.1, bf16[2,256,256]{2,1,0:T(8,128)(2,1)} %w_inlet.1, ...), custom_call_target="tpu_custom_call" | custom-call | tf_op jit(solution)/shard_map/pallas_call | solution.py:686
  61.7 3.2 %copy.13 = bf16[512,2048]{1,0:T(8,128)(2,1)} copy(bf16[512,2048]{1,0:T(8,128)(2,1)} %shard_map.109) | data formatting | bytes 4194304

commit v2 on v1

--- a/solution.py
+++ b/solution.py
@@ -14,12 +14,14 @@
 SEG = CHUNK // 8
 STRIDE = SEG + 8
 LANES = 128
-LAG = 2
-FIRST = 3
+LAG = 6
+FIRST = 1
 EVERY = 3
-BEHIND = 4
-AHEAD = 6
+BEHIND = 3
+AHEAD = 7
+EARLY = 3
 BETWEEN = 1
+REST = 4
 LN2 = math.log(2.0)
 GELU_A = math.sqrt(2.0 / math.pi)
 GELU_B = GELU_A * 0.044715
@@ -50,13 +52,15 @@
 
 def kernel(
     sizes,
-    tokens, in_gain, w_input, w_gate, taps, w_rate, w_inlet, decay_param, bias, out_gain, w_out,
+    tokens, in_gain_h, w_input, w_gate, taps_h, w_rate, w_inlet, decay_h, bias_h, out_gain_h, w_out,
     out,
+    in_gain, taps, decay_param, bias, out_gain, tail,
     x, w_in, w_all, gates_w, inv, proj, graw, conv, raw, bias_p, scale_row, before,
     state, prod, gate, pre_s, pre_p, natural, gated, arrived, total, result, halo,
     squares, squares_in, ends, ends_in,
     x_sem, w_sem, out_load_sem, halo_send, halo_recv, z_send, z_recv, y_send, y_recv,
     m_send, m_recv, end_send, end_recv, a_send, a_recv, q_send, q_recv, own_sem, out_sem,
+    small_sem, tail_sem,
 ):
     n_grp, n_sp, n_tp = sizes
     grp, sp, tp = lax.axis_index("grp"), lax.axis_index("sp"), lax.axis_index("tp")
@@ -95,6 +99,14 @@
         w_out, w_all.at[pl.ds(pl.multiple_of(sp * shard, shard), shard)], out_load_sem
     )
 
+    smalls = [
+        pltpu.make_async_copy(source, target, small_sem.at[n])
+        for n, (source, target) in enumerate((
+            (in_gain_h, in_gain), (w_rate, gates_w.at[:, :, 0:head]),
+            (w_inlet, gates_w.at[:, :, head : 2 * head]), (decay_h, decay_param),
+            (bias_h, bias), (taps_h, taps), (out_gain_h, out_gain),
+        ))
+    ]
     ends_in[...] = jnp.zeros_like(ends_in)
     barrier = pltpu.get_barrier_semaphore()
     for d in range(1, n_sp):
@@ -107,9 +119,17 @@
         )
     pl.semaphore_signal(barrier, inc=1, device_id={"grp": across}, device_id_type=MESH)
 
+    smalls[0].start()
     for copy in w_copies(0):
         copy.start()
+    halo_rows = halo.shape[0]
+    tail_copy = pltpu.make_async_copy(
+        tokens.at[pl.ds(rows - halo_rows, halo_rows)], tail, tail_sem
+    )
+    tail_copy.start()
     x_copy(0).start()
+    for copy in smalls[1:]:
+        copy.start()
 
     def remote(src, dst, send, recv, where):
         return pltpu.make_async_remote_copy(
@@ -117,9 +137,8 @@
             device_id=where, device_id_type=MESH,
         )
 
-    halo_rows = halo.shape[0]
     halo_copy = remote(
-        tokens.at[pl.ds(rows - halo_rows, halo_rows)], halo, halo_send, halo_recv,
+        tail, halo, halo_send, halo_recv,
         {"sp": jnp.minimum(sp + 1, n_sp - 1)},
     )
 
@@ -166,7 +185,7 @@
         from_left = jnp.where(b <= 2 * inner, b % 2 == 1, leftward)
         return jnp.where(from_left, sp - d, sp + d)
 
-    held = 2
+    held = (1, 2) if heads > 1 else ()
 
     def each_source(n, action):
         d, p = 1 + n // pieces, n % pieces
@@ -204,23 +223,15 @@
             each_source(n, take_z)
             each_source(n, functools.partial(send_on, False))
 
-        @pl.when((n >= held) & (n < items))
+        @pl.when(((n < min(held, default=0)) | (n > max(held, default=-1))) & (n < items))
         def _():
             each_source(n, functools.partial(send_on, True))
-
-        @pl.when(n == held)
-        def _():
-            for k in range(held):
-                each_source(k, functools.partial(send_on, True))
 
         @pl.when(n >= LAG)
         def _():
             each_source(n - LAG, take_y)
 
     def fold(h):
-        for copy in w_copies(h):
-            copy.wait()
-
         def block(j, _):
             at = pl.ds(pl.multiple_of(j * CHUNK, CHUNK), CHUNK)
             gain = columns_of(in_gain[0:1, at])
@@ -438,26 +449,32 @@
         lax.fori_loop(0, n_tp, owner, 0)
 
     h_all = range(heads)
-    for h in h_all:
-        gates_w[h, :, 0:head] = w_rate[h] * 0.5
-        gates_w[h, :, head : 2 * head] = w_inlet[h] * 0.5
-    scale_row[...] = softplus_of_minus(decay_param[...]) * (-4.0 / LN2)
-    fold(0)
-    x_copy(0).wait()
-    x_copy(1).start()
+    smalls[0].wait()
+    for copy in w_copies(0):
+        copy.wait()
     for h in range(1, heads):
         for copy in w_copies(h):
             copy.start()
-    acc, scale = project(0, True)
-    for c in range(parts):
-        proj[c, 7 * STRIDE + SEG : 8 * STRIDE, :] = jnp.zeros((8, LANES), F32)
-
+    x_copy(1).start()
+    fold(0)
+    tail_copy.wait()
     pl.semaphore_wait(barrier, n_sp - 1 + n_tp - 1 + 1)
     pl.when(sp < n_sp - 1)(halo_copy.start)
     for p in range(pieces):
         pl.when(sp < n_sp - 1)(own_copy(True, p).start)
         pl.when(sp > 0)(own_copy(False, p).start)
+    x_copy(0).wait()
+    acc, scale = project(0, True)
+    for c in range(parts):
+        proj[c, 7 * STRIDE + SEG : 8 * STRIDE, :] = jnp.zeros((8, LANES), F32)
+    for copy in smalls[1:]:
+        copy.wait()
+    for h in h_all:
+        gates_w[h] = gates_w[h] * 0.5
+    scale_row[...] = softplus_of_minus(decay_param[...]) * (-4.0 / LN2)
     for h in range(1, heads):
+        for copy in w_copies(h):
+            copy.wait()
         fold(h)
     for i in range(2, chunks):
         x_copy(i).start()
@@ -492,6 +509,13 @@
         if sums:
             x_copy(s + 2).wait()
 
+        if not sums and heads > 1:
+
+            @pl.when(s == chunks)
+            def _():
+                for k in held:
+                    each_source(k, functools.partial(send_on, True))
+
         @pl.when((s >= FIRST) & ((s - FIRST) % EVERY == 0))
         def _():
             pump((s - FIRST) // EVERY)
@@ -518,8 +542,7 @@
     carry = elementwise(steps - 1, carry)
     last = heads - 1
     send_ends(last, carry)
-    pump(done)
-    done += 1
+    before_last = min(done + EARLY, items + LAG)
 
     def pump_some(first, end):
         def one(n, _):
@@ -528,6 +551,8 @@
 
         lax.fori_loop(first, end, one, 0)
 
+    pump_some(done, before_last)
+    done = before_last
     phase_b(last, take_ends(last))
     out_load.wait()
 
@@ -588,9 +613,12 @@
     mates = {0}
     for index, (b, u) in enumerate(work):
         needed = b * pieces + LAG
-        if index >= n_sp - 1 and progressive:
-            needed = items + LAG
+        if index == n_sp - 1 and progressive:
+            needed = max(needed, items + LAG - REST)
         if b > 0:
+            pump_some(cursor, max(cursor, needed))
+            cursor = max(cursor, needed)
+        elif index > 0:
             pump_some(cursor, max(cursor, needed))
             cursor = max(cursor, needed)
         if b not in mates:
@@ -611,6 +639,29 @@
 
         lax.fori_loop(0, width // tile, partial_sum, 0)
         cursor = min(cursor + BETWEEN, items + LAG)
+    def drain_one(source, p, from_left):
+        onward(source, p, from_left, lambda copy: copy.wait_send())
+        y_copy(source, p).wait_send()
+        m_copy(source, p, False).wait_send()
+        m_copy(source, p, True).wait_send()
+
+    def drain(n, _):
+        each_source(n, drain_one)
+        return 0
+
+    drained = max(0, items + LAG - REST - LAG - 2)
+    pl.when(sp < n_sp - 1)(halo_copy.wait_send)
+    for p in range(pieces):
+        pl.when(sp < n_sp - 1)(own_copy(True, p).wait_send)
+        pl.when(sp > 0)(own_copy(False, p).wait_send)
+
+    for h in h_all:
+        for d in range(1, n_sp):
+            pl.when(sp + d < n_sp)(end_copy(h, d).wait_send)
+        for k in range(1, n_tp):
+            a_copy(h, k).wait_send()
+            q_copy(h, k).wait_send()
+    lax.fori_loop(0, drained, drain, 0)
     b = n_sp - 1
     if b > 0:
         pump_some(cursor, items + LAG)
@@ -639,28 +690,7 @@
 
     lax.fori_loop(0, width // tile, final, 0)
 
-    pl.when(sp < n_sp - 1)(halo_copy.wait_send)
-    for p in range(pieces):
-        pl.when(sp < n_sp - 1)(own_copy(True, p).wait_send)
-        pl.when(sp > 0)(own_copy(False, p).wait_send)
-
-    def drain_one(source, p, from_left):
-        onward(source, p, from_left, lambda copy: copy.wait_send())
-        y_copy(source, p).wait_send()
-        m_copy(source, p, False).wait_send()
-        m_copy(source, p, True).wait_send()
-
-    def drain(n, _):
-        each_source(n, drain_one)
-        return 0
-
-    lax.fori_loop(0, items, drain, 0)
-    for h in h_all:
-        for d in range(1, n_sp):
-            pl.when(sp + d < n_sp)(end_copy(h, d).wait_send)
-        for k in range(1, n_tp):
-            a_copy(h, k).wait_send()
-            q_copy(h, k).wait_send()
+    lax.fori_loop(drained, items, drain, 0)
     for n in range(width // tile):
         out_copy(n).wait()
 
@@ -681,14 +711,19 @@
     all_channels = channels * n_tp
     tile = 512 if out_width % 512 == 0 else 256
     hbm = pl.BlockSpec(memory_space=pl.ANY)
-    vmem = pl.BlockSpec(memory_space=pltpu.VMEM)
     dma = pltpu.SemaphoreType.DMA
     return pl.pallas_call(
         functools.partial(kernel, sizes),
         out_shape=jax.ShapeDtypeStruct((out_rows, out_width), BF16),
-        in_specs=[hbm, vmem, hbm, hbm, vmem, vmem, vmem, vmem, vmem, vmem, hbm],
+        in_specs=[hbm] * 11,
         out_specs=hbm,
         scratch_shapes=[
+            pltpu.VMEM((1, width), F32),
+            pltpu.VMEM(conv_taps.shape, F32),
+            pltpu.VMEM((1, channels), F32),
+            pltpu.VMEM((heads, rows), F32),
+            pltpu.VMEM((1, channels), F32),
+            pltpu.VMEM((16, width), BF16),
             pltpu.VMEM((rows, width), BF16),
             pltpu.VMEM((heads, width, 2 * head), BF16),
             pltpu.VMEM((all_channels, out_width), BF16),
@@ -735,6 +770,8 @@
             dma((heads * n_tp,)),
             dma((2 * heads,)),
             dma((out_width // tile,)),
+            dma((7,)),
+            dma,
         ],
         compiler_params=pltpu.CompilerParams(
             collective_id=0, has_side_effects=True, vmem_limit_bytes=62 * 1024 * 1024

time: 65.1 us -> 58.5 us (0.90); the launches traced: 64.9 us -> 57.5 us
  Pallas kernels: 61.7 us -> 54.3 us
    pallas_call x1, Pallas kernels: 61.7 us -> 54.3 us  [body(): pl.pallas_call(functools.partial(kernel, sizes), out_shape=jax.ShapeDtype...]
where the time goes in v2:
time: 58.5 us; the launch traced here: 57.5 us
  Pallas kernels  54.3 us (93%)
  local copies, waits for them, and re-layouts  3.16 us (5%)
    pallas_call x1, Pallas kernels, body(): pl.pallas_call(functools.partial(kernel, sizes), out_shape=jax.ShapeDtype...  54.3 us
    unnamed x1, local copies, waits for them, and re-layouts  3.16 us

profile of v2, /device:TPU:24, one launch (start us, length us, event | category | flops | bytes accessed | tf_op | source)
XLA Modules:
  0.0 57.5 jit_solution(10316673982219211360)
XLA Ops:
  0.0 54.3 %shard_map.109 = bf16[512,2048]{1,0:T(8,128)(2,1)} custom-call(bf16[2048,2048]{1,0:T(8,128)(2,1)} %tokens.1, f32[1,2048]{1,0:T(1,128)} %bitcast.3, bf16[2048,512]{1,0:T(8,128)(2,1)} %w_input.1, bf16[2048,512]{1,0:T(8,128)(2,1)} %w_gate.1, f32[4,512]{1,0:T(4,128)} %taps_h.1, bf16[2,256,256]{2,1,0:T(8,128)(2,1)} %w_rate.1, bf16[2,256,256]{2,1,0:T(8,128)(2,1)} %w_inlet.1, ...), custom_call_target="tpu_custom_call" | custom-call | tf_op jit(solution)/shard_map/pallas_call | solution.py:715
  54.3 3.2 %copy.13 = bf16[512,2048]{1,0:T(8,128)(2,1)} copy(bf16[512,2048]{1,0:T(8,128)(2,1)} %shard_map.109) | data formatting | bytes 4194304

commit v3 on v2

--- a/solution.py
+++ b/solution.py
@@ -56,10 +56,10 @@
     out,
     in_gain, taps, decay_param, bias, out_gain, tail,
     x, w_in, w_all, gates_w, inv, proj, graw, conv, raw, bias_p, scale_row, before,
-    state, prod, gate, pre_s, pre_p, natural, gated, arrived, total, result, halo,
+    state, prod, gate, pre_s, pre_p, natural, gated, arrived, total, halo,
     squares, squares_in, ends, ends_in,
     x_sem, w_sem, out_load_sem, halo_send, halo_recv, z_send, z_recv, y_send, y_recv,
-    m_send, m_recv, end_send, end_recv, a_send, a_recv, q_send, q_recv, own_sem, out_sem,
+    m_send, m_recv, end_send, end_recv, a_send, a_recv, q_send, q_recv, own_sem,
     small_sem, tail_sem,
 ):
     n_grp, n_sp, n_tp = sizes
@@ -152,30 +152,28 @@
     def own_copy(to_right, p):
         mine = which_of(False, core)
         first = pl.multiple_of(mine * quarter + p * piece, piece)
-        slot = ((0 if to_right else 1) * n_sp + sp) * pieces + p
         return remote(
             w_out.at[pl.ds(first, piece)], w_rows(sp, mine, p),
-            z_send.at[slot], z_recv.at[sp * pieces + p],
+            z_send.at[0 if to_right else 1], z_recv.at[sp * pieces + p],
             {"sp": jnp.minimum(sp + 1, n_sp - 1) if to_right else jnp.maximum(sp - 1, 0)},
         )
 
     def z_copy(source, p, to_right):
         at = w_rows(source, which_of(False, core), p)
-        slot = ((0 if to_right else 1) * n_sp + source) * pieces + p
         return remote(
-            at, at, z_send.at[slot], z_recv.at[source * pieces + p],
+            at, at, z_send.at[0 if to_right else 1], z_recv.at[source * pieces + p],
             {"sp": jnp.minimum(sp + 1, n_sp - 1) if to_right else jnp.maximum(sp - 1, 0)},
         )
 
     def y_copy(source, p, incoming=False):
         at = w_rows(source, which_of(incoming, core), p)
         slot = source * pieces + p
-        return remote(at, at, y_send.at[slot], y_recv.at[slot], {"grp": across})
+        return remote(at, at, y_send, y_recv.at[slot], {"grp": across})
 
     def m_copy(source, p, second, incoming=False):
         at = w_rows(source, which_of(second, 1 - core if incoming else core), p)
         slot = ((1 if second else 0) * n_sp + source) * pieces + p
-        return remote(at, at, m_send.at[slot], m_recv.at[slot], {"tp": mate})
+        return remote(at, at, m_send, m_recv.at[slot], {"tp": mate})
 
     inner = jnp.minimum(sp, n_sp - 1 - sp)
     leftward = sp > n_sp - 1 - sp
@@ -639,29 +637,17 @@
 
         lax.fori_loop(0, width // tile, partial_sum, 0)
         cursor = min(cursor + BETWEEN, items + LAG)
-    def drain_one(source, p, from_left):
-        onward(source, p, from_left, lambda copy: copy.wait_send())
-        y_copy(source, p).wait_send()
-        m_copy(source, p, False).wait_send()
-        m_copy(source, p, True).wait_send()
-
-    def drain(n, _):
-        each_source(n, drain_one)
-        return 0
-
-    drained = max(0, items + LAG - REST - LAG - 2)
+    def all_sent(semaphore, quarters):
+        at = w_all.at[pl.ds(0, quarters * quarter)]
+        remote(at, at, semaphore, semaphore, {"grp": across}).wait_send()
+
     pl.when(sp < n_sp - 1)(halo_copy.wait_send)
-    for p in range(pieces):
-        pl.when(sp < n_sp - 1)(own_copy(True, p).wait_send)
-        pl.when(sp > 0)(own_copy(False, p).wait_send)
-
     for h in h_all:
         for d in range(1, n_sp):
             pl.when(sp + d < n_sp)(end_copy(h, d).wait_send)
         for k in range(1, n_tp):
             a_copy(h, k).wait_send()
             q_copy(h, k).wait_send()
-    lax.fori_loop(0, drained, drain, 0)
     b = n_sp - 1
     if b > 0:
         pump_some(cursor, items + LAG)
@@ -674,25 +660,22 @@
     out_scale = lax.rsqrt(row[0:1] / (n_tp * heads * head) + 1e-06)
     scale_cols = jnp.broadcast_to(out_scale, (LANES, out_rows)).T
 
-    def out_copy(n):
-        columns = columns_at(n)
-        return pltpu.make_async_copy(result.at[:, columns], out.at[:, columns], out_sem.at[n])
-
     def final(n, _):
         columns = columns_at(n)
         value = multiply(source, columns, tuple(range(units)))
         if n_sp > 1:
             value = value + total[:, columns]
         value = value * jnp.concatenate([scale_cols] * (tile // LANES), axis=1)
-        result[:, columns] = value.astype(BF16)
-        out_copy(n).start()
+        out[:, columns] = value.astype(BF16)
         return 0
 
     lax.fori_loop(0, width // tile, final, 0)
 
-    lax.fori_loop(drained, items, drain, 0)
-    for n in range(width // tile):
-        out_copy(n).wait()
+    for k in range(n_sp - 1):
+        pl.when(sp == k)(functools.partial(all_sent, z_send.at[0], k + 1))
+        pl.when(sp == n_sp - 1 - k)(functools.partial(all_sent, z_send.at[1], k + 1))
+    all_sent(y_send, n_sp - 1)
+    all_sent(m_send, 2 * (n_sp - 1))
 
 
 def body(sizes, tokens, in_gain, w_input, w_gate, conv_taps, w_rate, w_inlet, decay_param,
@@ -709,14 +692,13 @@
     quarter = shard // (2 * n_grp)
     pieces = quarter // max(16, quarter // 4)
     all_channels = channels * n_tp
-    tile = 512 if out_width % 512 == 0 else 256
     hbm = pl.BlockSpec(memory_space=pl.ANY)
     dma = pltpu.SemaphoreType.DMA
     return pl.pallas_call(
         functools.partial(kernel, sizes),
-        out_shape=jax.ShapeDtypeStruct((out_rows, out_width), BF16),
+        out_shape=pltpu.VMEM((out_rows, out_width), BF16),
         in_specs=[hbm] * 11,
-        out_specs=hbm,
+        out_specs=pl.BlockSpec(memory_space=pltpu.VMEM),
         scratch_shapes=[
             pltpu.VMEM((1, width), F32),
             pltpu.VMEM(conv_taps.shape, F32),
@@ -745,7 +727,6 @@
             pltpu.VMEM((heads, rows, head), BF16),
             pltpu.VMEM((n_tp * heads, out_rows, head), BF16),
             pltpu.VMEM((out_rows, out_width), F32),
-            pltpu.VMEM((out_rows, out_width), BF16),
             pltpu.VMEM((16, width), BF16),
             pltpu.VMEM((heads * n_tp, 8, out_rows), F32),
             pltpu.VMEM((n_tp * heads, 8, out_rows), F32),
@@ -756,11 +737,11 @@
             dma,
             dma,
             dma,
-            dma((2 * n_sp * pieces,)),
+            dma((2,)),
             dma((n_sp * pieces,)),
+            dma,
             dma((n_sp * pieces,)),
-            dma((n_sp * pieces,)),
-            dma((2 * n_sp * pieces,)),
+            dma,
             dma((2 * n_sp * pieces,)),
             dma((heads * n_sp,)),
             dma((heads * n_sp,)),
@@ -769,17 +750,19 @@
             dma((heads * n_tp,)),
             dma((heads * n_tp,)),
             dma((2 * heads,)),
-            dma((out_width // tile,)),
             dma((7,)),
             dma,
         ],
         compiler_params=pltpu.CompilerParams(
-            collective_id=0, has_side_effects=True, vmem_limit_bytes=62 * 1024 * 1024
+            collective_id=0, has_side_effects=True, vmem_limit_bytes=58 * 1024 * 1024
         ),
-    )(
-        tokens, in_gain.reshape(1, width), w_input, w_gate, conv_taps, w_rate, w_inlet,
-        decay_param.reshape(1, channels), decay_bias, out_gain.reshape(1, channels), w_out,
-    )
+    )(*(
+        pltpu.with_memory_space_constraint(array, pltpu.HBM)
+        for array in (
+            tokens, in_gain.reshape(1, width), w_input, w_gate, conv_taps, w_rate, w_inlet,
+            decay_param.reshape(1, channels), decay_bias, out_gain.reshape(1, channels), w_out,
+        )
+    ))
 
 
 def solution(mesh):

time: 58.5 us -> 54.9 us (0.938)
  local copies, waits for them, and re-layouts: 3.16 us -> 1.32 us
  Pallas kernels: 54.3 us -> 52.6 us
    unnamed x1, local copies, waits for them, and re-layouts: 3.16 us -> 1.32 us
    pallas_call x1, Pallas kernels: 54.3 us -> 52.6 us  [body(): pl.pallas_call(functools.partial(kernel, sizes), out_shape=pltpu.VMEM((ou...]
where the time goes in v3:
time: 54.9 us; the launch traced here: 53.9 us
  Pallas kernels  52.6 us (96%)
  local copies, waits for them, and re-layouts  1.32 us (2%)
    pallas_call x1, Pallas kernels, body(): pl.pallas_call(functools.partial(kernel, sizes), out_shape=pltpu.VMEM((ou...  52.6 us
    unnamed x1, local copies, waits for them, and re-layouts  1.32 us

profile of v3, /device:TPU:24, one launch (start us, length us, event | category | flops | bytes accessed | tf_op | source)
XLA Modules:
  0.0 53.9 jit_solution(15418819196578026940)
XLA Ops:
  0.0 52.6 %shard_map.109 = bf16[512,2048]{1,0:T(8,128)(2,1)S(1)} custom-call(bf16[2048,2048]{1,0:T(8,128)(2,1)} %tokens.1, f32[1,2048]{1,0:T(1,128)} %bitcast.3, bf16[2048,512]{1,0:T(8,128)(2,1)} %w_input.1, bf16[2048,512]{1,0:T(8,128)(2,1)} %w_gate.1, f32[4,512]{1,0:T(4,128)} %taps_h.1, bf16[2,256,256]{2,1,0:T(8,128)(2,1)} %w_rate.1, bf16[2,256,256]{2,1,0:T(8,128)(2,1)} %w_inlet.1, ...), custom_call_target="tpu_custom_call" | custom-call | tf_op jit(solution)/shard_map/pallas_call | solution.py:697
  52.6 1.3 %copy.13 = bf16[512,2048]{1,0:T(8,128)(2,1)} copy(bf16[512,2048]{1,0:T(8,128)(2,1)S(1)} %shard_map.109) | data formatting | bytes 4194304

commit v4 on v3

--- a/solution.py
+++ b/solution.py
@@ -18,7 +18,7 @@
 FIRST = 1
 EVERY = 3
 BEHIND = 3
-AHEAD = 7
+AHEAD = 8
 EARLY = 3
 BETWEEN = 1
 REST = 4
@@ -81,6 +81,9 @@
     core = lax.rem(tp, 2)
     mate = tp + 1 - 2 * core
     across = 1 - grp
+    side = lax.rem(tp // 2, 2)
+    beside = tp + 2 - 4 * side
+    over_tp = 0
 
     def x_copy(i):
         at = pl.ds(pl.multiple_of(i * CHUNK, CHUNK), CHUNK)
@@ -146,11 +149,15 @@
         first = source * shard + which * quarter + p * piece
         return w_all.at[pl.ds(pl.multiple_of(first, piece), piece)]
 
-    def which_of(other, owner):
-        return (across if other else grp) * 2 + owner
+    def is_over_tp(source, p):
+        return (p < over_tp) & (source > 0) & (source < n_sp - 1)
+
+    def which_of(source, p, other, owner):
+        near = jnp.where(is_over_tp(source, p), side, grp)
+        return (1 - near if other else near) * 2 + owner
 
     def own_copy(to_right, p):
-        mine = which_of(False, core)
+        mine = which_of(sp, p, False, core)
         first = pl.multiple_of(mine * quarter + p * piece, piece)
         return remote(
             w_out.at[pl.ds(first, piece)], w_rows(sp, mine, p),
@@ -159,19 +166,21 @@
         )
 
     def z_copy(source, p, to_right):
-        at = w_rows(source, which_of(False, core), p)
+        at = w_rows(source, which_of(source, p, False, core), p)
         return remote(
             at, at, z_send.at[0 if to_right else 1], z_recv.at[source * pieces + p],
             {"sp": jnp.minimum(sp + 1, n_sp - 1) if to_right else jnp.maximum(sp - 1, 0)},
         )
 
     def y_copy(source, p, incoming=False):
-        at = w_rows(source, which_of(incoming, core), p)
+        at = w_rows(source, which_of(source, p, incoming, core), p)
         slot = source * pieces + p
-        return remote(at, at, y_send, y_recv.at[slot], {"grp": across})
+        turn = is_over_tp(source, p)
+        to = {"grp": jnp.where(turn, grp, across), "tp": jnp.where(turn, beside, tp)}
+        return remote(at, at, y_send, y_recv.at[slot], to)
 
     def m_copy(source, p, second, incoming=False):
-        at = w_rows(source, which_of(second, 1 - core if incoming else core), p)
+        at = w_rows(source, which_of(source, p, second, 1 - core if incoming else core), p)
         slot = ((1 if second else 0) * n_sp + source) * pieces + p
         return remote(at, at, m_send, m_recv.at[slot], {"tp": mate})
 
@@ -184,6 +193,7 @@
         return jnp.where(from_left, sp - d, sp + d)
 
     held = (1, 2) if heads > 1 else ()
+    late = (4,) if heads > 1 else ()
 
     def each_source(n, action):
         d, p = 1 + n // pieces, n % pieces
@@ -221,7 +231,10 @@
             each_source(n, take_z)
             each_source(n, functools.partial(send_on, False))
 
-        @pl.when(((n < min(held, default=0)) | (n > max(held, default=-1))) & (n < items))
+        at_once = (n < min(held, default=0)) | (n > max(held, default=-1))
+        at_once &= (n < min(late, default=0)) | (n > max(late, default=-1))
+
+        @pl.when(at_once & (n < items))
         def _():
             each_source(n, functools.partial(send_on, True))
 
@@ -230,15 +243,19 @@
             each_source(n - LAG, take_y)
 
     def fold(h):
+        together = 4 if width % (4 * CHUNK) == 0 else 1
+
         def block(j, _):
-            at = pl.ds(pl.multiple_of(j * CHUNK, CHUNK), CHUNK)
-            gain = columns_of(in_gain[0:1, at])
-            for c in range(2 * parts):
-                lanes = slice(c * LANES, (c + 1) * LANES)
-                w_in[h, at, lanes] = (w_in[h, at, lanes].astype(F32) * gain).astype(BF16)
+            for k in range(together):
+                first = pl.multiple_of((j * together + k) * CHUNK, CHUNK)
+                at = pl.ds(first, CHUNK)
+                gain = columns_of(in_gain[0:1, at])
+                for c in range(2 * parts):
+                    lanes = slice(c * LANES, (c + 1) * LANES)
+                    w_in[h, at, lanes] = (w_in[h, at, lanes].astype(F32) * gain).astype(BF16)
             return 0
 
-        lax.fori_loop(0, width // CHUNK, block, 0)
+        lax.fori_loop(0, width // (together * CHUNK), block, 0)
 
     def norm_of(chunk):
         as_float = chunk.astype(F32)
@@ -509,6 +526,12 @@
 
         if not sums and heads > 1:
 
+            @pl.when((s >= chunks) & (s % chunks == BEHIND))
+            def _():
+                phase_b(s // chunks - 1, take_ends(s // chunks - 1))
+
+        if not sums and heads > 1:
+
             @pl.when(s == chunks)
             def _():
                 for k in held:
@@ -517,12 +540,6 @@
         @pl.when((s >= FIRST) & ((s - FIRST) % EVERY == 0))
         def _():
             pump((s - FIRST) // EVERY)
-
-        if not sums and heads > 1:
-
-            @pl.when((s >= chunks) & (s % chunks == BEHIND))
-            def _():
-                phase_b(s // chunks - 1, take_ends(s // chunks - 1))
 
         acc, scale = project(s + 2, sums)
         carry = elementwise(s, carry)
@@ -541,6 +558,8 @@
     last = heads - 1
     send_ends(last, carry)
     before_last = min(done + EARLY, items + LAG)
+    for k in late:
+        each_source(k, functools.partial(send_on, True))
 
     def pump_some(first, end):
         def one(n, _):
@@ -579,8 +598,7 @@
 
         lax.fori_loop(0, pieces, one, 0)
 
-    def prepare(b, h):
-        source = source_of(b)
+    def prepare(source, h):
         if progressive:
             wait_from(lax.rem(tp - source + n_tp, n_tp), h)
         return source
@@ -604,6 +622,15 @@
             for h in h_all:
                 wait_from(k, h)
     units = shard // deep
+    end = source_of(n_sp - 1)
+    base = 2 * (tp // 2)
+    end_at = lax.rem(end - base + n_sp, n_sp) if progressive else 0
+
+    def source_for(b, u):
+        if u == 0 or not progressive:
+            return source_of(b)
+        return lax.rem(base + jnp.where(b < end_at, b, b + 1), n_sp)
+
     work = [(b, u) for u in range(units) for b in range(n_sp - 1)]
     ahead = max(done, AHEAD * items // 12)
     pump_some(done, ahead)
@@ -622,7 +649,7 @@
         if b not in mates:
             wait_mate(b)
             mates.add(b)
-        source = prepare(b, u)
+        source = prepare(source_for(b, u), u)
 
         def partial_sum(n, _, source=source, index=index, u=u, cursor=cursor):
             columns = columns_at(n)
@@ -653,7 +680,7 @@
         pump_some(cursor, items + LAG)
         wait_mate(b)
     for u in range(units):
-        source = prepare(b, u)
+        source = prepare(source_of(b), u)
     row = squares_in[0]
     for k in range(1, n_tp * heads):
         row = row + squares_in[k]

time: 54.9 us -> 54.1 us (0.985)
  no operation moved by 1% of the time
where the time goes in v4:
time: 54.1 us; the launch traced here: 53.4 us
  Pallas kernels  52.1 us (96%)
  local copies, waits for them, and re-layouts  1.32 us (2%)
    pallas_call x1, Pallas kernels, body(): pl.pallas_call(functools.partial(kernel, sizes), out_shape=pltpu.VMEM((ou...  52.1 us
    unnamed x1, local copies, waits for them, and re-layouts  1.32 us

profile of v4, /device:TPU:24, one launch (start us, length us, event | category | flops | bytes accessed | tf_op | source)
XLA Modules:
  0.0 53.4 jit_solution(3559513937700131901)
XLA Ops:
  0.0 52.1 %shard_map.109 = bf16[512,2048]{1,0:T(8,128)(2,1)S(1)} custom-call(bf16[2048,2048]{1,0:T(8,128)(2,1)} %tokens.1, f32[1,2048]{1,0:T(1,128)} %bitcast.3, bf16[2048,512]{1,0:T(8,128)(2,1)} %w_input.1, bf16[2048,512]{1,0:T(8,128)(2,1)} %w_gate.1, f32[4,512]{1,0:T(4,128)} %taps_h.1, bf16[2,256,256]{2,1,0:T(8,128)(2,1)} %w_rate.1, bf16[2,256,256]{2,1,0:T(8,128)(2,1)} %w_inlet.1, ...), custom_call_target="tpu_custom_call" | custom-call | tf_op jit(solution)/shard_map/pallas_call | solution.py:724
  52.1 1.3 %copy.13 = bf16[512,2048]{1,0:T(8,128)(2,1)} copy(bf16[512,2048]{1,0:T(8,128)(2,1)S(1)} %shard_map.109) | data formatting | bytes 4194304
